TPU v7x, 32 devices: a whole 2x2x4 slice. The times are simulated.
32 devices in a mesh: fs: 4 (over z), rep: 4 (over y, x), tp: 2 (over core).
Axes of the slice: x: 2, y: 2, z: 4, core: 2. Of those that a mesh axis runs over, the one named last changes fastest.
Arguments:
- saved_inputs: bfloat16 [12288, 2048], P(('fs', 'rep')), may hold values from -6 to 6
- query_cotangent: bfloat16 [12288, 1024], P(('fs', 'rep'), 'tp'), may hold values from -0.053955078 to 0.053955078
- value_cotangent: bfloat16 [12288, 2048], P(('fs', 'rep'), 'tp'), may hold values from -0.053955078 to 0.053955078
- query_weight: float32 [2048, 1024], P('fs', 'tp'), may hold values from -0.125 to 0.125
- value_weight: float32 [2048, 2048], P('fs', 'tp'), may hold values from -0.125 to 0.125
- query_factor: bfloat16 [2048, 256], P('fs'), as said below
- value_factor: bfloat16 [2048, 256], P('fs'), as said below
- query_first: float32 [256, 1024], P('rep', 'tp'), may hold values from -6 to 6
- query_second: float32 [256, 1024], P('rep', 'tp'), may hold values from 0.3 to 3
- value_first: float32 [256, 2048], P('rep', 'tp'), may hold values from -6 to 6
- value_second: float32 [256, 2048], P('rep', 'tp'), may hold values from 0.3 to 3
Outputs:
- query_direction: float32 [2048, 1024], P('fs', 'tp')
- value_direction: float32 [2048, 2048], P('fs', 'tp')
- query_master: float32 [2048, 1024], P('fs', 'tp')
- value_master: float32 [2048, 2048], P('fs', 'tp')
- query_first_new: float32 [256, 1024], P('rep', 'tp')
- query_second_new: float32 [256, 1024], P('rep', 'tp')
- value_first_new: float32 [256, 2048], P('rep', 'tp')
- value_second_new: float32 [256, 2048], P('rep', 'tp')
- query_copy: bfloat16 [2048, 1024], P(None, 'tp')
- value_copy: bfloat16 [2048, 2048], P(None, 'tp')
Inputs may be any that keep to these rules, and one draw needn't show every extreme that they name: `query_factor`: A matrix of full rank. `value_factor`: A matrix of full rank.
All inputs are finite; a program needn't handle non-finite values.
Results may differ from a plain program's by a relative error of at most 0.012.
Values may be sent and summed in bfloat16 or wider, within the bound.
A program may use at most 128 MiB of HBM per device.

v0:
```python
import jax
import jax.numpy as jnp
from jax import lax
from jax.sharding import PartitionSpec as P

D = 2048
QK = 1024
VW = 2048


BETA_ONE = 0.8
BETA_TWO = 0.9
EPS_RATIO = 1e-08
EPS_NORM = 1e-06
RATE = 0.02


def moments(projected, first, second):
    first_new = BETA_ONE * first + (1.0 - BETA_ONE) * projected
    second_new = BETA_TWO * second + (1.0 - BETA_TWO) * projected * projected
    ratio = first_new / (jnp.sqrt(second_new) + EPS_RATIO)
    return (first_new, second_new, ratio)


def local(
    saved_inputs,
    query_cotangent,
    value_cotangent,
    query_weight,
    value_weight,
    query_factor,
    value_factor,
    query_first,
    query_second,
    value_first,
    value_second,
):
    query_cols = query_cotangent.shape[1]
    both_cot = jnp.concatenate([query_cotangent, value_cotangent], axis=1)
    dims = (((0,), (0,)), ((), ()))
    highest = lax.Precision.HIGHEST
    grads = lax.dot_general(saved_inputs, both_cot, dims, preferred_element_type=jnp.float32)
    first_term = jnp.dot(
        lax.all_gather(query_factor, "fs", axis=0, tiled=True).astype(jnp.float32).T,
        grads[:, :query_cols],
        precision=highest,
    )
    second_term = jnp.dot(
        lax.all_gather(value_factor, "fs", axis=0, tiled=True).astype(jnp.float32).T,
        grads[:, query_cols:],
        precision=highest,
    )
    proj_query = first_term
    proj_value = second_term
    proj_query, proj_value = (
        lax.psum_scatter(
            proj_query.astype(jnp.bfloat16), "rep", scatter_dimension=0, tiled=True
        ).astype(jnp.float32),
        lax.psum_scatter(
            proj_value.astype(jnp.bfloat16), "rep", scatter_dimension=0, tiled=True
        ).astype(jnp.float32),
    )
    proj_query, proj_value = lax.psum((proj_query, proj_value), "fs")
    query_first_new, query_second_new, query_ratio = moments(proj_query, query_first, query_second)
    value_first_new, value_second_new, value_ratio = moments(proj_value, value_first, value_second)
    query_ratio, value_ratio = (
        lax.all_gather(query_ratio, "rep", axis=0, tiled=True),
        lax.all_gather(value_ratio, "rep", axis=0, tiled=True),
    )
    query_raw = jnp.dot(query_factor.astype(jnp.float32), query_ratio, precision=highest)
    value_raw = jnp.dot(value_factor.astype(jnp.float32), value_ratio, precision=highest)
    query_total, value_total = lax.psum(
        (jnp.sum(query_raw * query_raw), jnp.sum(value_raw * value_raw)), ("fs", "tp")
    )
    query_direction = query_raw * lax.rsqrt(query_total / (D * QK) + EPS_NORM)
    value_direction = value_raw * lax.rsqrt(value_total / (D * VW) + EPS_NORM)
    query_master = query_weight - RATE * query_direction
    value_master = value_weight - RATE * value_direction
    query_copy, value_copy = (
        lax.all_gather(query_master.astype(jnp.bfloat16), "fs", axis=0, tiled=True),
        lax.all_gather(value_master.astype(jnp.bfloat16), "fs", axis=0, tiled=True),
    )
    return (
        query_direction,
        value_direction,
        query_master,
        value_master,
        query_first_new,
        query_second_new,
        value_first_new,
        value_second_new,
        query_copy,
        value_copy,
    )


def solution(mesh):
    placed = (
        P(("fs", "rep"), None),
        P(("fs", "rep"), "tp"),
        P(("fs", "rep"), "tp"),
        P("fs", "tp"),
        P("fs", "tp"),
        P("fs", None),
        P("fs", None),
        P("rep", "tp"),
        P("rep", "tp"),
        P("rep", "tp"),
        P("rep", "tp"),
    )
    return jax.shard_map(
        local,
        mesh=mesh,
        in_specs=placed,
        out_specs=(
            P("fs", "tp"),
            P("fs", "tp"),
            P("fs", "tp"),
            P("fs", "tp"),
            P("rep", "tp"),
            P("rep", "tp"),
            P("rep", "tp"),
            P("rep", "tp"),
            P(None, "tp"),
            P(None, "tp"),
        ),
        check_vma=False,
    )
```

profile of v0, /device:TPU:24, one launch (start us, length us, event | category | flops | bytes accessed | tf_op | source)
XLA Modules:
  0.0 337.9 jit_solution(9919645747390022899)
XLA Ops:
  7.2 0.7 all-gather.6.cloned.1.call-update
  8.0 0.7 all-gather.8.cloned.1.call-update
  8.7 0.3 copy-done
  9.1 9.6 %convolution_bitcast_fusion = f32[2048,1536]{0,1:T(8,128)} fusion(bf16[768,2048]{1,0:T(8,128)(2,1)S(1)} %copy-done, bf16[768,1024]{1,0:T(8,128)(2,1)} %param.13, bf16[768,512]{1,0:T(8,128)(2,1)} %param.12), kind=kOutput, calls=%fused_computation | convolution fusion | flops 4836556800 | bytes 18087936 | tf_op jit(solution)/shard_map/dot_general | solution.py:42
  18.7 18.3 %all-gather.6.cloned.1.call-done = bf16[2048,256]{1,0:T(8,128)(2,1)} async-done(((bf16[512,256]{1,0:T(8,128)(2,1)}), bf16[2048,256]{1,0:T(8,128)(2,1)}) %all-gather.6.cloned.1.call-update) | async-done | bytes 1048592 | tf_op jit(solution)/shard_map/all_gather | solution.py:44
  37.0 4.5 %fusion.16 = bf16[256,512]{0,1:T(8,128)(2,1)S(1)} fusion(bf16[2048,256]{1,0:T(8,128)(2,1)} %all-gather.6.cloned.1.call-done, f32[2048,1536]{0,1:T(8,128)} %convolution_bitcast_fusion), kind=kOutput, calls=%fused_computation.14 | convolution fusion | flops 3221356544 | bytes 5505024 | tf_op jit(solution)/shard_map/dot_general | solution.py:43
  41.5 0.8 copy.65
  42.4 23.5 %all-gather.8.cloned.1.call-done = bf16[2048,256]{1,0:T(8,128)(2,1)} async-done(((bf16[512,256]{1,0:T(8,128)(2,1)}), bf16[2048,256]{1,0:T(8,128)(2,1)}) %all-gather.8.cloned.1.call-update) | async-done | bytes 1048592 | tf_op jit(solution)/shard_map/all_gather | solution.py:49
  66.0 8.2 %fusion.10 = bf16[256,1024]{0,1:T(8,128)(2,1)} fusion(bf16[2048,256]{1,0:T(8,128)(2,1)} %all-gather.8.cloned.1.call-done, f32[2048,1536]{0,1:T(8,128)} %convolution_bitcast_fusion), kind=kOutput, calls=%fused_computation.12 | convolution fusion | flops 6442713088 | bytes 9961472 | tf_op jit(solution)/shard_map/dot_general | solution.py:48
  74.2 2.0 copy.67
  76.3 18.3 %reduce-scatter.7.cloned.1.call-done = bf16[64,512]{1,0:T(8,128)(2,1)} async-done(((bf16[256,512]{1,0:T(8,128)(2,1)}), bf16[64,512]{1,0:T(8,128)(2,1)}) %reduce-scatter.7.cloned.1.call-update) | async-done | bytes 65552 | tf_op jit(solution)/shard_map/reduce_scatter | solution.py:56
  94.6 28.4 %reduce-scatter.9.cloned.1.call-done = bf16[64,1024]{1,0:T(8,128)(2,1)} async-done(((bf16[256,1024]{1,0:T(8,128)(2,1)}), bf16[64,1024]{1,0:T(8,128)(2,1)}) %reduce-scatter.9.cloned.1.call-update) | async-done | bytes 131088 | tf_op jit(solution)/shard_map/reduce_scatter | solution.py:59
  123.0 23.5 %all-reduce.3 = (f32[64,512]{1,0:T(8,128)}, f32[64,1024]{1,0:T(8,128)}) all-reduce(bf16[64,512]{1,0:T(8,128)(2,1)} %reduce-scatter.7.cloned.1.call-done, bf16[64,1024]{1,0:T(8,128)(2,1)} %reduce-scatter.9.cloned.1.call-done), channel_id=1, replica_groups=mesh['fs'=4,'rep'=4,'tp'=2] {'fs'}, use_global_device_ids=true, to_apply=%region_1.0 | all-reduce | flops 98304 | bytes 589824 | tf_op jit(solution)/shard_map/psum | solution.py:63
  146.5 2.0 add_divide_fusion
  148.5 2.6 copy.57
  151.1 1.7 add_divide_fusion.1
  152.9 11.2 %all_gather.19 = f32[256,512]{1,0:T(8,128)S(1)} all-gather(f32[64,512]{1,0:T(8,128)S(1)} %get-tuple-element.53), channel_id=1, replica_groups=mesh['fs'=4,'rep'=4,'tp'=2] {'rep'}, dimensions={0}, use_global_device_ids=true | all-gather | bytes 655360 | tf_op jit(solution)/shard_map/all_gather | solution.py:67
  164.0 3.5 %multiply_reduce_fusion.1 = (f32[]{:T(128)}, f32[512,512]{1,0:T(8,128)}) fusion(f32[256,512]{1,0:T(8,128)S(1)} %all_gather.19, bf16[512,256]{1,0:T(8,128)(2,1)} %param.16), kind=kOutput, calls=%fused_computation.17 | convolution fusion | flops 805830656 | bytes 1835012 | tf_op jit(solution)/shard_map/dot_general | solution.py:70
  167.6 9.8 %all-gather.10.cloned.1.call-done = f32[256,1024]{1,0:T(8,128)} async-done(((f32[64,1024]{1,0:T(8,128)}), f32[256,1024]{1,0:T(8,128)}) %all-gather.10.cloned.1.call-update) | async-done | bytes 1048592 | tf_op jit(solution)/shard_map/all_gather | solution.py:68
  177.3 5.0 %multiply_reduce_fusion = (f32[]{:T(128)}, f32[1024,512]{1,0:T(8,128)}) fusion(f32[256,1024]{1,0:T(8,128)} %all-gather.10.cloned.1.call-done, bf16[512,256]{1,0:T(8,128)(2,1)S(1)} %copy-done.1), kind=kOutput, calls=%fused_computation.10 | convolution fusion | flops 1611661312 | bytes 3407876 | tf_op jit(solution)/shard_map/dot_general | solution.py:71
  182.3 11.4 %all-reduce = (f32[]{:T(128)}, f32[]{:T(128)}) all-reduce(f32[]{:T(128)} %get-tuple-element.56, f32[]{:T(128)} %get-tuple-element.58), channel_id=1, replica_groups=mesh['fs'=4,'rep'=4,'tp'=2] {'fs','tp'}, use_global_device_ids=true, to_apply=%region_3.0 | all-reduce | flops 2 | bytes 16 | tf_op jit(solution)/shard_map/psum | solution.py:72
  194.4 3.4 %fusion.23 = (bf16[512,512]{0,1:T(8,128)(2,1)}, f32[512,512]{0,1:T(8,128)}, f32[512,512]{0,1:T(8,128)}) fusion(f32[512,512]{0,1:T(8,128)} %copy.57, f32[512,512]{1,0:T(8,128)} %get-tuple-element.57, f32[]{:T(128)S(6)} %rsqrt.6), kind=kLoop, calls=%fused_computation.28 | loop fusion | flops 1048576 | bytes 4718596 | tf_op jit(solution)/shard_map/convert_element_type | solution.py:80
  197.9 2.9 copy.58
  201.5 5.4 %fusion.22 = (bf16[512,1024]{0,1:T(8,128)(2,1)}, f32[512,1024]{0,1:T(8,128)}, f32[512,1024]{0,1:T(8,128)}) fusion(f32[512,1024]{0,1:T(8,128)} %copy.58, f32[1024,512]{1,0:T(8,128)} %get-tuple-element.59, f32[]{:T(128)S(6)} %rsqrt.7), kind=kLoop, calls=%fused_computation.27 | loop fusion | flops 2097152 | bytes 9437188 | tf_op jit(solution)/shard_map/convert_element_type | solution.py:81
  206.8 3.0 copy.60
  209.8 2.9 copy.62
  212.7 2.5 copy.59
  215.2 2.5 copy.61
  217.8 26.5 %all-gather.12.cloned.1.call-done = bf16[2048,512]{0,1:T(8,128)(2,1)} async-done(((bf16[512,512]{0,1:T(8,128)(2,1)}), bf16[2048,512]{0,1:T(8,128)(2,1)}) %all-gather.12.cloned.1.call-update) | async-done | bytes 2097168 | tf_op jit(solution)/shard_map/all_gather | solution.py:80
  244.3 3.9 %copy.63 = bf16[2048,512]{1,0:T(8,128)(2,1)} copy(bf16[2048,512]{0,1:T(8,128)(2,1)} %all-gather.12.cloned.1.call-done) | data formatting | bytes 4194304
  248.2 76.4 %all-gather.14.cloned.1.call-done = bf16[2048,1024]{0,1:T(8,128)(2,1)} async-done(((bf16[512,1024]{0,1:T(8,128)(2,1)}), bf16[2048,1024]{0,1:T(8,128)(2,1)}) %all-gather.14.cloned.1.call-update) | async-done | bytes 4194320 | tf_op jit(solution)/shard_map/all_gather | solution.py:81
  324.6 6.4 %copy.64 = bf16[2048,1024]{1,0:T(8,128)(2,1)} copy(bf16[2048,1024]{0,1:T(8,128)(2,1)} %all-gather.14.cloned.1.call-done) | data formatting | bytes 8388608
  (19 shorter events, 0.4 us)
Async XLA Ops:
  7.2 1.9 copy-start
  7.2 29.8 %all-gather.6.cloned.1.call-start = ((), (), s32[]{:S(2)}) async-start(), calls=%async_computation.2 | async-start | bytes 1310720 | tf_op jit(solution)/shard_map/all_gather | solution.py:44
  7.9 58.1 %all-gather.8.cloned.1.call-start = ((), (), s32[]{:S(2)}) async-start(), calls=%async_computation.3 | async-start | bytes 1310720 | tf_op jit(solution)/shard_map/all_gather | solution.py:49
  8.7 85.9 %reduce-scatter.7.cloned.1.call-start = ((), (), s32[]{:S(2)}) async-start(), calls=%async_computation.7 | async-start | bytes 327680 | tf_op jit(solution)/shard_map/reduce_scatter | solution.py:56
  42.4 104.1 %copy-start.2 = (f32[64,1024]{1,0:T(8,128)S(1)}, f32[64,1024]{1,0:T(8,128)}, u32[]{:S(2)}) copy-start(f32[64,1024]{1,0:T(8,128)} %param.21) | copy-start | bytes 786436
  42.4 80.6 %reduce-scatter.9.cloned.1.call-start = ((), (), s32[]{:S(2)}) async-start(), calls=%async_computation.8 | async-start | bytes 655360 | tf_op jit(solution)/shard_map/reduce_scatter | solution.py:59
  76.2 74.9 %copy-start.3 = (f32[64,512]{1,0:T(8,128)S(1)}, f32[64,512]{1,0:T(8,128)}, u32[]{:S(2)}) copy-start(f32[64,512]{1,0:T(8,128)} %param.19) | copy-start | bytes 393220
  76.3 101.0 %all-gather.10.cloned.1.call-start = ((), (), s32[]{:S(2)}) async-start(), calls=%async_computation.4 | async-start | bytes 1310720 | tf_op jit(solution)/shard_map/all_gather | solution.py:68
  148.5 28.8 %copy-start.1 = (bf16[512,256]{1,0:T(8,128)(2,1)S(1)}, bf16[512,256]{1,0:T(8,128)(2,1)}, u32[]{:S(2)}) copy-start(bf16[512,256]{1,0:T(8,128)(2,1)} %param.17) | copy-start | bytes 786436
  148.5 95.8 %all-gather.12.cloned.1.call-start = ((), (), s32[]{:S(2)}) async-start(), calls=%async_computation.5 | async-start | bytes 2621440 | tf_op jit(solution)/shard_map/all_gather | solution.py:80
  197.8 126.8 %all-gather.14.cloned.1.call-start = ((), (), s32[]{:S(2)}) async-start(), calls=%async_computation.6 | async-start | bytes 5242880 | tf_op jit(solution)/shard_map/all_gather | solution.py:81
Sparse Core Ops, SparseCore 0:
  9.6 27.4 all-gather.5
  38.6 27.3 all-gather.7
  69.3 25.2 reduce-scatter.6
  97.8 25.1 reduce-scatter.8
  148.6 28.6 all-gather.9
  198.0 46.2 all-gather.11
  245.9 78.7 all-gather.13
where the time goes:
time: 343 us; the launch traced here: 338 us
  waiting for transfers between devices  203 us (59%)
  blocking collectives  46.1 us (13%)
  matrix products  30.8 us (9%)
  local copies, waits for them, and re-layouts  29.9 us (9%)
  between operations  15.6 us (5%)
  other arithmetic  12.5 us (4%)
    all_gather x1, waiting for transfers between devices, local(): lax.all_gather(value_master.astype(jnp.bfloat16), 'fs', axis=0, tiled=True)  76.4 us
    unnamed x18, local copies, waits for them, and re-layouts  29.9 us
    reduce_scatter x1, waiting for transfers between devices, local(): lax.psum_scatter(proj_value.astype(jnp.bfloat16), 'rep', scatter_dimensio...  28.4 us
    all_gather x1, waiting for transfers between devices, local(): lax.all_gather(query_master.astype(jnp.bfloat16), 'fs', axis=0, tiled=True)  26.5 us
    all_gather x1, waiting for transfers between devices, local(): lax.all_gather(value_factor, 'fs', axis=0, tiled=True).astype(jnp.float32)  23.5 us
    psum x1, blocking collectives, local(): proj_query, proj_value = lax.psum((proj_query, proj_value), 'fs')  23.5 us
    all_gather x1, waiting for transfers between devices, local(): lax.all_gather(query_factor, 'fs', axis=0, tiled=True).astype(jnp.float32)  18.3 us
    reduce_scatter x1, waiting for transfers between devices, local(): lax.psum_scatter(proj_query.astype(jnp.bfloat16), 'rep', scatter_dimensio...  18.3 us
  transfers between devices with their start and end apart: 7, of which 7 were waited for; matrix products, arithmetic and copies ran while one was open for 17% of the time, Pallas kernels for 0%

commit v1 on v0

v1 whole, which is shorter than its diff:
```python
import jax
import jax.numpy as jnp
from jax import lax
from jax.sharding import PartitionSpec as P

BETA_ONE = 0.8
BETA_TWO = 0.9
EPS_RATIO = 1e-08
EPS_NORM = 1e-06
RATE = 0.02


def moments(projected, first, second):
    first_new = BETA_ONE * first + (1.0 - BETA_ONE) * projected
    second_new = BETA_TWO * second + (1.0 - BETA_TWO) * projected * projected
    ratio = first_new / (jnp.sqrt(second_new) + EPS_RATIO)
    return (first_new, second_new, ratio)


def local(
    saved_inputs,
    query_cotangent,
    value_cotangent,
    query_weight,
    value_weight,
    query_factor,
    value_factor,
    query_first,
    query_second,
    value_first,
    value_second,
):
    qc = query_cotangent.shape[1]
    rank = query_factor.shape[1]
    rows = query_weight.shape[0]
    tp = lax.axis_size("tp")
    bf = jnp.bfloat16
    f32 = jnp.float32
    dims = (((0,), (0,)), ((), ()))
    factors = lax.all_gather(
        jnp.concatenate([query_factor, value_factor], axis=1), "fs", axis=0, tiled=True
    )
    weights = lax.all_gather(
        jnp.concatenate([query_weight.astype(bf), value_weight.astype(bf)], axis=1),
        "fs",
        axis=0,
        tiled=True,
    )
    low = jnp.dot(saved_inputs, factors, preferred_element_type=f32).astype(bf)
    proj = jnp.concatenate(
        [
            lax.dot_general(low[:, :rank], query_cotangent, dims, preferred_element_type=f32),
            lax.dot_general(low[:, rank:], value_cotangent, dims, preferred_element_type=f32),
        ],
        axis=1,
    )
    proj = lax.psum_scatter(proj.astype(bf), "rep", scatter_dimension=0, tiled=True)
    proj = lax.psum(proj.astype(f32), "fs")
    query_first_new, query_second_new, query_ratio = moments(
        proj[:, :qc], query_first, query_second
    )
    value_first_new, value_second_new, value_ratio = moments(
        proj[:, qc:], value_first, value_second
    )
    ratio = jnp.concatenate([query_ratio.astype(bf), value_ratio.astype(bf)], axis=1)
    ratio = lax.all_gather(ratio, "rep", axis=0, tiled=True)
    query_raw = jnp.dot(factors[:, :rank], ratio[:, :qc], preferred_element_type=f32)
    value_raw = jnp.dot(factors[:, rank:], ratio[:, qc:], preferred_element_type=f32)
    query_total, value_total = lax.psum(
        (jnp.sum(query_raw * query_raw), jnp.sum(value_raw * value_raw)), "tp"
    )
    query_scale = lax.rsqrt(query_total / (query_raw.size * tp) + EPS_NORM)
    value_scale = lax.rsqrt(value_total / (value_raw.size * tp) + EPS_NORM)
    query_copy = (weights[:, :qc].astype(f32) - RATE * (query_raw * query_scale)).astype(bf)
    value_copy = (weights[:, qc:].astype(f32) - RATE * (value_raw * value_scale)).astype(bf)
    start = lax.axis_index("fs") * rows
    query_direction = lax.dynamic_slice_in_dim(query_raw, start, rows, 0) * query_scale
    value_direction = lax.dynamic_slice_in_dim(value_raw, start, rows, 0) * value_scale
    query_master = query_weight - RATE * query_direction
    value_master = value_weight - RATE * value_direction
    return (
        query_direction,
        value_direction,
        query_master,
        value_master,
        query_first_new,
        query_second_new,
        value_first_new,
        value_second_new,
        query_copy,
        value_copy,
    )


def solution(mesh):
    return jax.shard_map(
        local,
        mesh=mesh,
        in_specs=(
            P(("fs", "rep"), None),
            P(("fs", "rep"), "tp"),
            P(("fs", "rep"), "tp"),
            P("fs", "tp"),
            P("fs", "tp"),
            P("fs", None),
            P("fs", None),
            P("rep", "tp"),
            P("rep", "tp"),
            P("rep", "tp"),
            P("rep", "tp"),
        ),
        out_specs=(
            P("fs", "tp"),
            P("fs", "tp"),
            P("fs", "tp"),
            P("fs", "tp"),
            P("rep", "tp"),
            P("rep", "tp"),
            P("rep", "tp"),
            P("rep", "tp"),
            P(None, "tp"),
            P(None, "tp"),
        ),
        check_vma=False,
    )
```

time: 343 us -> 285 us (0.83)
  local copies, waits for them, and re-layouts: 29.9 us -> 0.03 us
  waiting for transfers between devices: 203 us -> 186 us
  matrix products: 30.8 us -> 14.4 us
  other arithmetic: 12.5 us -> 27 us
  blocking collectives: 46.1 us -> 37.5 us
    unnamed x18 -> x12, local copies, waits for them, and re-layouts: 29.9 us -> 0.03 us
    reduce_scatter x2 -> x1, waiting for transfers between devices: 46.7 us -> 27 us  [local(): lax.psum_scatter(proj.astype(bf), 'rep', scatter_dimension=0, tiled=True)]
    dot_general x5, matrix products: 30.8 us -> 14.4 us  [the longest x1 6.09 us: local(): jnp.dot(factors[:, rank:], ratio[:, qc:], preferred_element_type=f32)]
    psum x1, blocking collectives: 11.4 us -> 3.08 us  [local(): lax.psum((jnp.sum(query_raw * query_raw), jnp.sum(value_raw * value_raw))...]
    sub x0 -> x2, other arithmetic: none -> 8.21 us  [the longest x1 4.56 us: local(): value_master = value_weight - RATE * value_direction]
    convert_element_type x2 -> x4, other arithmetic: 8.76 us -> 14.6 us  [the longest x1 5.67 us: local(): (weights[:, qc:].astype(f32) - RATE * (value_raw * value_scale)).astype(bf)]
    all_gather x5 -> x2, waiting for transfers between devices: 155 us -> 159 us  [the longest x1 113 us: local(): lax.all_gather(jnp.concatenate([query_weight.astype(bf), value_weight.ast...]
    concatenate x0 -> x4, other arithmetic: none -> 4.2 us  [the longest x1 2.01 us: local(): jnp.concatenate([query_factor, value_factor], axis=1)]
  transfers between devices with their start and end apart: 7 -> 3, of which waited for: 7 -> 3; matrix products, arithmetic and copies ran while one was open for 17% -> 0% of each run, Pallas kernels for 0% -> 0%
where the time goes in v1:
time: 285 us; the launch traced here: 280 us
  waiting for transfers between devices  186 us (65%)
  blocking collectives  37.5 us (13%)
  other arithmetic  27 us (9%)
  between operations  15.2 us (5%)
  matrix products  14.4 us (5%)
    all_gather x1, waiting for transfers between devices, local(): lax.all_gather(jnp.concatenate([query_weight.astype(bf), value_weight.ast...  113 us
    all_gather x1, waiting for transfers between devices, local(): lax.all_gather(jnp.concatenate([query_factor, value_factor], axis=1), 'fs...  45.5 us
    reduce_scatter x1, waiting for transfers between devices, local(): lax.psum_scatter(proj.astype(bf), 'rep', scatter_dimension=0, tiled=True)  27 us
    psum x1, blocking collectives, local(): proj = lax.psum(proj.astype(f32), 'fs')  23.4 us
    all_gather x1, blocking collectives, local(): ratio = lax.all_gather(ratio, 'rep', axis=0, tiled=True)  11 us
    dot_general x1, matrix products, local(): jnp.dot(factors[:, rank:], ratio[:, qc:], preferred_element_type=f32)  6.09 us
  transfers between devices with their start and end apart: 3, of which 3 were waited for; matrix products, arithmetic and copies ran while one was open for 0% of the time, Pallas kernels for 0%

profile of v1, /device:TPU:24, one launch (start us, length us, event | category | flops | bytes accessed | tf_op | source)
XLA Modules:
  0.0 280.2 jit_solution(16459601803138328107)
XLA Ops:
  7.2 0.0 copy-start
  7.2 0.0 all-gather.3.cloned.1.call-start
  7.2 2.0 pad_maximum_fusion.2
  9.2 0.0 all-gather.3.cloned.1.call-update
  9.3 0.0 reduce-scatter.2.cloned.1.call-start
  9.3 45.5 %all-gather.3.cloned.1.call-done = bf16[2048,512]{1,0:T(8,128)(2,1)} async-done(((bf16[512,512]{1,0:T(8,128)(2,1)}), bf16[2048,512]{1,0:T(8,128)(2,1)}) %all-gather.3.cloned.1.call-update) | async-done | bytes 2097168 | tf_op jit(solution)/shard_map/all_gather | solution.py:40
  54.9 0.0 copy-done
  54.9 3.6 %fusion = bf16[768,512]{0,1:T(8,128)(2,1)S(1)} fusion(bf16[2048,512]{1,0:T(8,128)(2,1)} %all-gather.3.cloned.1.call-done, bf16[768,2048]{1,0:T(8,128)(2,1)S(1)} %copy-done), kind=kOutput, calls=%fused_computation.8 | convolution fusion | flops 1611005952 | bytes 6029312 | tf_op jit(solution)/shard_map/dot_general | solution.py:49
  58.5 0.0 copy-done.4
  58.5 0.6 convolution_convert_fusion.1
  59.0 0.0 copy-done.5
  59.1 0.4 convolution_convert_fusion.2
  59.4 0.9 pad_maximum_fusion.1
  60.4 0.0 reduce-scatter.2.cloned.1.call-update
  60.4 0.0 all-gather.5.cloned.1.call-start
  60.4 27.0 %reduce-scatter.2.cloned.1.call-done = bf16[64,1536]{1,0:T(8,128)(2,1)} async-done(((bf16[256,1536]{1,0:T(8,128)(2,1)}), bf16[64,1536]{1,0:T(8,128)(2,1)}) %reduce-scatter.2.cloned.1.call-update) | async-done | bytes 196624 | tf_op jit(solution)/shard_map/reduce_scatter | solution.py:57
  87.4 23.4 %all-reduce.2 = f32[64,1536]{1,0:T(8,128)S(1)} all-reduce(bf16[64,1536]{1,0:T(8,128)(2,1)} %reduce-scatter.2.cloned.1.call-done), channel_id=1, replica_groups=mesh['fs'=4,'rep'=4,'tp'=2] {'fs'}, use_global_device_ids=true, to_apply=%region_1.0 | all-reduce | flops 98304 | bytes 589824 | tf_op jit(solution)/shard_map/psum | solution.py:58
  110.9 2.1 divide_convert_fusion
  113.0 1.7 divide_convert_fusion.1
  114.7 11.0 %all_gather.10 = bf16[256,1536]{1,0:T(8,128)(2,1)S(1)} all-gather(bf16[64,1536]{1,0:T(8,128)(2,1)S(1)} %pad_maximum_fusion.3), channel_id=1, replica_groups=mesh['fs'=4,'rep'=4,'tp'=2] {'rep'}, dimensions={0}, use_global_device_ids=true | all-gather | bytes 983040 | tf_op jit(solution)/shard_map/all_gather | solution.py:66
  125.8 0.0 copy-done.2
  125.8 3.8 %multiply_reduce_fusion.1 = (f32[]{:T(128)}, f32[2048,512]{1,0:T(8,128)}) fusion(bf16[256,1536]{1,0:T(8,128)(2,1)S(1)} %all_gather.10, bf16[2048,512]{1,0:T(8,128)(2,1)S(1)} %copy-done.2), kind=kOutput, calls=%fused_computation.3 | convolution fusion | flops 538968064 | bytes 5505028 | tf_op jit(solution)/shard_map/dot_general | solution.py:67
  129.5 6.1 %multiply_reduce_fusion = (f32[]{:T(128)}, f32[2048,1024]{1,0:T(8,128)}) fusion(bf16[256,1536]{1,0:T(8,128)(2,1)S(1)} %all_gather.10, bf16[2048,512]{1,0:T(8,128)(2,1)S(1)} %copy-done.2), kind=kOutput, calls=%fused_computation.1 | convolution fusion | flops 1077936128 | bytes 9961476 | tf_op jit(solution)/shard_map/dot_general | solution.py:68
  135.6 3.1 %all-reduce = (f32[]{:T(128)}, f32[]{:T(128)}) all-reduce(f32[]{:T(128)} %get-tuple-element.24, f32[]{:T(128)} %get-tuple-element.26), channel_id=1, replica_groups=mesh['fs'=4,'rep'=4,'tp'=2] {'tp'}, use_global_device_ids=true, to_apply=%region_3.0 | all-reduce | flops 2 | bytes 16 | tf_op jit(solution)/shard_map/psum | solution.py:69
  140.1 0.0 copy-start.3
  140.1 3.6 %multiply_subtract_fusion.1 = (f32[512,512]{1,0:T(8,128)}, f32[512,512]{1,0:T(8,128)}, bf16[512,512]{1,0:T(8,128)(2,1)S(1)}) fusion(f32[512,512]{1,0:T(8,128)} %param.14, f32[]{:T(128)S(6)} %rsqrt.6, f32[2048,512]{1,0:T(8,128)} %get-tuple-element.25, s32[]{:T(128)S(6)} %select_n.4), kind=kLoop, calls=%fused_computation.15 | loop fusion | flops 1048576 | bytes 4718600 | tf_op jit(solution)/shard_map/sub | solution.py:79
  143.8 4.6 %multiply_subtract_fusion = (f32[512,1024]{1,0:T(8,128)}, f32[512,1024]{1,0:T(8,128)}, bf16[512,1024]{1,0:T(8,128)(2,1)S(1)}) fusion(f32[512,1024]{1,0:T(8,128)S(1)} %copy-done.3, f32[]{:T(128)S(6)} %rsqrt.7, f32[2048,1024]{1,0:T(8,128)} %get-tuple-element.27, s32[]{:T(128)S(6)} %select_n.4), kind=kLoop, calls=%fused_computation.4 | loop fusion | flops 2097152 | bytes 9437192 | tf_op jit(solution)/shard_map/sub | solution.py:80
  148.3 1.2 pad_maximum_fusion
  149.6 0.0 all-gather.5.cloned.1.call-update
  149.6 113.4 %all-gather.5.cloned.1.call-done = bf16[2048,1536]{1,0:T(8,128)(2,1)} async-done(((bf16[512,1536]{1,0:T(8,128)(2,1)}), bf16[2048,1536]{1,0:T(8,128)(2,1)}) %all-gather.5.cloned.1.call-update) | async-done | bytes 6291472 | tf_op jit(solution)/shard_map/all_gather | solution.py:43
  263.0 5.1 %subtract_convert_fusion.1 = bf16[2048,512]{1,0:T(8,128)(2,1)} fusion(f32[2048,512]{1,0:T(8,128)} %get-tuple-element.25, bf16[2048,1536]{1,0:T(8,128)(2,1)} %all-gather.5.cloned.1.call-done, f32[]{:T(128)S(6)} %rsqrt.6), kind=kLoop, calls=%fused_computation.2 | loop fusion | flops 5242880 | bytes 8388612 | tf_op jit(solution)/shard_map/convert_element_type | solution.py:74
  268.0 5.7 %subtract_convert_fusion = bf16[2048,1024]{1,0:T(8,128)(2,1)} fusion(f32[2048,1024]{1,0:T(8,128)} %get-tuple-element.27, bf16[2048,1536]{1,0:T(8,128)(2,1)S(1)} %copy-done.1, f32[]{:T(128)S(6)} %rsqrt.7), kind=kLoop, calls=%fused_computation | loop fusion | flops 10485760 | bytes 16777220 | tf_op jit(solution)/shard_map/convert_element_type | solution.py:75
  (7 shorter events, 0.0 us)
Async XLA Ops:
  7.2 47.7 %copy-start = (bf16[768,2048]{1,0:T(8,128)(2,1)S(1)}, bf16[768,2048]{1,0:T(8,128)(2,1)}, u32[]{:S(2)}) copy-start(bf16[768,2048]{1,0:T(8,128)(2,1)} %param.11) | copy-start | bytes 9437188
  7.2 47.7 %all-gather.3.cloned.1.call-start = ((), (), s32[]{:S(2)}) async-start(), calls=%async_computation.1 | async-start | bytes 2621440 | tf_op jit(solution)/shard_map/all_gather | solution.py:40
  9.3 78.1 %reduce-scatter.2.cloned.1.call-start = ((), (), s32[]{:S(2)}) async-start(), calls=%async_computation.2 | async-start | bytes 983040 | tf_op jit(solution)/shard_map/reduce_scatter | solution.py:57
  54.9 3.6 %copy-start.4 = (bf16[768,1024]{1,0:T(8,128)(2,1)S(1)}, bf16[768,1024]{1,0:T(8,128)(2,1)}, u32[]{:S(2)}) copy-start(bf16[768,1024]{1,0:T(8,128)(2,1)} %param.13) | copy-start | bytes 4718596
  54.9 4.2 %copy-start.5 = (bf16[768,512]{1,0:T(8,128)(2,1)S(1)}, bf16[768,512]{1,0:T(8,128)(2,1)}, u32[]{:S(2)}) copy-start(bf16[768,512]{1,0:T(8,128)(2,1)} %param.12) | copy-start | bytes 2359300
  60.4 202.6 %all-gather.5.cloned.1.call-start = ((), (), s32[]{:S(2)}) async-start(), calls=%async_computation.3 | async-start | bytes 7864320 | tf_op jit(solution)/shard_map/all_gather | solution.py:43
  110.8 14.9 %copy-start.2 = (bf16[2048,512]{1,0:T(8,128)(2,1)S(1)}, bf16[2048,512]{1,0:T(8,128)(2,1)}, u32[]{:S(2)}) copy-start(bf16[2048,512]{1,0:T(8,128)(2,1)} %all-gather.3.cloned.1.call-done) | copy-start | bytes 6291460
  140.1 3.7 %copy-start.3 = (f32[512,1024]{1,0:T(8,128)S(1)}, f32[512,1024]{1,0:T(8,128)}, u32[]{:S(2)}) copy-start(f32[512,1024]{1,0:T(8,128)} %param.15) | copy-start | bytes 6291460
  263.0 5.1 %copy-start.1 = (bf16[2048,1536]{1,0:T(8,128)(2,1)S(1)}, bf16[2048,1536]{1,0:T(8,128)(2,1)}, u32[]{:S(2)}) copy-start(bf16[2048,1536]{1,0:T(8,128)(2,1)} %all-gather.5.cloned.1.call-done) | copy-start | bytes 18874372
Sparse Core Ops, SparseCore 0:
  10.1 44.6 all-gather.2
  60.5 26.8 reduce-scatter.1
  149.7 113.1 all-gather.4

commit v2 on v1

v2 whole, which is shorter than its diff:
```python
import functools

import jax
import jax.numpy as jnp
from jax import lax
from jax.experimental import pallas as pl
from jax.experimental.pallas import tpu as pltpu
from jax.sharding import PartitionSpec as P

BETA_ONE = 0.8
BETA_TWO = 0.9
EPS_RATIO = 1e-08
EPS_NORM = 1e-06
RATE = 0.02
BF = jnp.bfloat16
F32 = jnp.float32


def moments(projected, first, second):
    first_new = BETA_ONE * first + (1.0 - BETA_ONE) * projected
    second_new = BETA_TWO * second + (1.0 - BETA_TWO) * projected * projected
    ratio = first_new / (jnp.sqrt(second_new) + EPS_RATIO)
    return (first_new, second_new, ratio)


def exchange(
    nz,
    nr,
    x_hbm,
    cq_hbm,
    cv_hbm,
    wq_hbm,
    wv_hbm,
    qf_hbm,
    vf_hbm,
    q1_ref,
    q2_ref,
    v1_ref,
    v2_ref,
    w_out,
    f_ref,
    ratio_ref,
    first_out,
    second_out,
    scale_out,
    x_ref,
    cq_ref,
    cv_ref,
    wf_ref,
    wb_ref,
    low_ref,
    part_ref,
    rs_ref,
    z_ref,
    sq_ref,
    local_sem,
    f1_s,
    f1_r,
    w1_s,
    w1_r,
    f2_s,
    f2_r,
    w2_s,
    w2_r,
    rs_s,
    rs_r,
    zs_s,
    zs_r,
    ag_s,
    ag_r,
    tp_s,
    tp_r,
):
    z = lax.axis_index("fs")
    r = lax.axis_index("rep")
    t = lax.axis_index("tp")
    rows = qf_hbm.shape[0]
    part = rows // nr
    qc = cq_ref.shape[1]
    cols = w_out.shape[1]
    half = cols // 2
    width = w_out.shape[0]
    rank = low_ref.shape[2]
    own = rank // nr
    tokens = x_ref.shape[0]
    z_of = [lax.rem(z + k, nz) for k in range(nz)]
    z_from = [lax.rem(z + nz - k, nz) for k in range(nz)]
    r_of = [lax.rem(r + j, nr) for j in range(nr)]
    side = r + 1 - 2 * lax.rem(r, 2)
    over = lax.rem(r + 2, nr)
    corner = nr - 1 - r
    other = 1 - t

    def remote(src, dst, ss, rs, dev):
        return pltpu.make_async_remote_copy(
            src_ref=src,
            dst_ref=dst,
            send_sem=ss,
            recv_sem=rs,
            device_id=dev,
            device_id_type=pl.DeviceIdType.MESH,
        )

    def slab(zz, rr):
        return pl.ds(pl.multiple_of(zz * rows + rr * part, part), part)

    def fac_copy(src):
        return pltpu.make_async_copy(
            src,
            f_ref.at[t, pl.ds(pl.multiple_of(z * rows, rows), rows)],
            local_sem.at[0],
        )

    @pl.when(t == 0)
    def _():
        fac_copy(qf_hbm).start()

    @pl.when(t == 1)
    def _():
        fac_copy(vf_hbm).start()

    wq_in = pltpu.make_async_copy(wq_hbm, wf_ref.at[:, pl.ds(0, qc)], local_sem.at[1])
    wv_in = pltpu.make_async_copy(wv_hbm, wf_ref.at[:, pl.ds(qc, cols - qc)], local_sem.at[2])
    x_in = pltpu.make_async_copy(x_hbm, x_ref, local_sem.at[3])
    cq_in = pltpu.make_async_copy(cq_hbm, cq_ref, local_sem.at[4])
    cv_in = pltpu.make_async_copy(cv_hbm, cv_ref, local_sem.at[5])
    for c in (wq_in, wv_in, x_in, cq_in, cv_in):
        c.start()

    barrier = pltpu.get_barrier_semaphore()
    peers = [(z_of[k], r, t) for k in range(1, nz)]
    peers += [(z, r_of[j], t) for j in range(1, nr)]
    peers += [(z, r, other)]
    for dev in peers:
        pl.semaphore_signal(
            barrier, inc=1, device_id=dev, device_id_type=pl.DeviceIdType.MESH
        )
    pl.semaphore_wait(barrier, len(peers))

    fac_copy(qf_hbm).wait()
    sends = []
    f1 = []
    for k in range(1, nz):
        here = f_ref.at[t, slab(z, r)]
        c = remote(here, here, f1_s.at[k - 1], f1_r.at[k - 1], (z_of[k], r, t))
        c.start()
        f1.append(c)
    wq_in.wait()
    wv_in.wait()
    wb_ref[...] = wf_ref[...].astype(BF)
    w1 = []
    for k in range(1, nz):
        c = remote(
            wb_ref.at[pl.ds(pl.multiple_of(r * part, part), part)],
            w_out.at[slab(z, r)],
            w1_s.at[k - 1],
            w1_r.at[k - 1],
            (z_of[k], r, t),
        )
        c.start()
        w1.append(c)
    w_own = pltpu.make_async_copy(
        wb_ref, w_out.at[pl.ds(pl.multiple_of(z * rows, rows), rows)], local_sem.at[6]
    )
    w_own.start()

    f2 = []
    for k in range(1, nz):
        f1[k - 1].wait_recv()
        there = f_ref.at[t, slab(z_from[k], r)]
        for j in range(1, nr):
            n = (k - 1) * (nr - 1) + j - 1
            c = remote(there, there, f2_s.at[n], f2_r.at[n], (z, r_of[j], t))
            c.start()
            f2.append(c)
    for c in f2:
        c.wait_recv()
    fx = remote(f_ref.at[t], f_ref.at[t], tp_s.at[0], tp_r.at[0], (z, r, other))
    fx.start()
    x_in.wait()
    tile = tokens // 3

    @pl.loop(0, 3)
    def _(i):
        span = pl.ds(pl.multiple_of(i * tile, tile), tile)
        low_ref[t, span] = jnp.dot(
            x_ref[span, :], f_ref[t], preferred_element_type=F32
        ).astype(BF)

    lx = remote(low_ref.at[t], low_ref.at[t], tp_s.at[1], tp_r.at[1], (z, r, other))
    lx.start()
    cq_in.wait()
    cv_in.wait()
    lx.wait_recv()
    dims = (((0,), (0,)), ((), ()))
    part_ref[:, :qc] = lax.dot_general(
        low_ref[0], cq_ref[...], dims, preferred_element_type=F32
    ).astype(BF)
    part_ref[:, qc:] = lax.dot_general(
        low_ref[1], cv_ref[...], dims, preferred_element_type=F32
    ).astype(BF)

    def low_rows(rr):
        return pl.ds(pl.multiple_of(rr * own, own), own)

    rsc = []
    for j in range(1, nr):
        c = remote(
            part_ref.at[low_rows(r_of[j])],
            rs_ref.at[j - 1],
            rs_s.at[j - 1],
            rs_r.at[j - 1],
            (z, r_of[j], t),
        )
        c.start()
        rsc.append(c)

    w2 = {}

    def spread(k):
        w1[k - 1].wait_recv()
        there = w_out.at[slab(z_from[k], r)]
        for n, dev in ((0, side), (1, over)):
            c = remote(there, there, w2_s.at[k - 1, n], w2_r.at[k - 1, n], (z, dev, t))
            c.start()
            w2[k, n] = c

    def relay(k):
        for n, src, dev, at in ((0, side, over, 0), (1, over, side, half)):
            w2[k, n].wait_recv()
            there = w_out.at[slab(z_from[k], src), pl.ds(at, half)]
            c = remote(
                there, there, w2_s.at[k - 1, 2 + n], w2_r.at[k - 1, 2 + n], (z, dev, t)
            )
            c.start()
            w2[k, 2 + n] = c

    stages = [[], [], []]
    for k in range(1, nz):
        stages[min(k - 1, 2)].append(k)
    for c in rsc:
        c.wait_recv()
    total = part_ref[low_rows(r), :].astype(F32)
    for j in range(1, nr):
        total = total + rs_ref[j - 1].astype(F32)
    z_ref[z] = total.astype(BF)
    zc = []
    for k in range(1, nz):
        c = remote(z_ref.at[z], z_ref.at[z], zs_s.at[k - 1], zs_r.at[k - 1], (z_of[k], r, t))
        c.start()
        zc.append(c)
    for k in stages[0]:
        spread(k)
    for c in zc:
        c.wait_recv()
    proj = z_ref[0].astype(F32)
    for k in range(1, nz):
        proj = proj + z_ref[k].astype(F32)
    q1, q2, qr = moments(proj[:, :qc], q1_ref[...], q2_ref[...])
    v1, v2, vr = moments(proj[:, qc:], v1_ref[...], v2_ref[...])
    ratio_ref[low_rows(r), :qc] = qr.astype(BF)
    ratio_ref[low_rows(r), qc:] = vr.astype(BF)
    agc = []
    for j in range(1, nr):
        here = ratio_ref.at[low_rows(r)]
        c = remote(here, here, ag_s.at[j - 1], ag_r.at[j - 1], (z, r_of[j], t))
        c.start()
        agc.append(c)
    first_out[:, :qc] = q1
    first_out[:, qc:] = v1
    second_out[:, :qc] = q2
    second_out[:, qc:] = v2
    for k in stages[0]:
        relay(k)
    for k in stages[1]:
        spread(k)
    for k in stages[1]:
        relay(k)
    for k in stages[2]:
        spread(k)
    fx.wait_recv()
    for c in agc:
        c.wait_recv()
    step = min(256, width)

    def squares(i, acc):
        span = pl.ds(pl.multiple_of(i * step, step), step)
        a = jnp.dot(f_ref[0, span], ratio_ref[:, :qc], preferred_element_type=F32)
        b = jnp.dot(f_ref[1, span], ratio_ref[:, qc:], preferred_element_type=F32)
        a = jnp.sum(a * a, axis=0, keepdims=True)
        b = jnp.sum(b * b, axis=0, keepdims=True)
        return (acc[0] + a, acc[1] + b)

    qs, vs = lax.fori_loop(
        0,
        width // step,
        squares,
        (jnp.zeros((1, qc), F32), jnp.zeros((1, cols - qc), F32)),
    )
    qs = jnp.sum(qs, axis=1, keepdims=True)
    vs = jnp.sum(vs, axis=1, keepdims=True)
    row = lax.broadcasted_iota(jnp.int32, sq_ref.shape[1:], 0)
    sq_ref[t] = jnp.where(row == 0, qs / (width * qc * 2), vs / (width * (cols - qc) * 2))
    sx = remote(sq_ref.at[t], sq_ref.at[t], tp_s.at[2], tp_r.at[2], (z, r, other))
    sx.start()
    sx.wait_recv()
    scale_out[...] = lax.rsqrt(sq_ref[0] + sq_ref[1] + EPS_NORM)
    for k in stages[2]:
        relay(k)
    for k in range(1, nz):
        w2[k, 2].wait_recv()
        w2[k, 3].wait_recv()
    for c in f1 + w1 + f2 + rsc + zc + agc + [fx, lx, sx] + list(w2.values()):
        c.wait_send()
    w_own.wait()


def run_exchange(nz, nr, x, cq, cv, wq, wv, qf, vf, q1, q2, v1, v2):
    tokens, width = x.shape
    qc = cq.shape[1]
    cols = qc + cv.shape[1]
    rows, rank = qf.shape
    own = rank // nr
    any_spec = pl.BlockSpec(memory_space=pl.ANY)
    vmem = pl.BlockSpec(memory_space=pltpu.VMEM)
    dma = pltpu.SemaphoreType.DMA
    shape = jax.ShapeDtypeStruct
    return pl.pallas_call(
        functools.partial(exchange, nz, nr),
        out_shape=(
            shape((width, cols), BF),
            shape((2, width, rank), BF),
            shape((rank, cols), BF),
            shape((own, cols), F32),
            shape((own, cols), F32),
            shape((8, 128), F32),
        ),
        in_specs=[any_spec] * 7 + [vmem] * 4,
        out_specs=(any_spec, vmem, vmem, vmem, vmem, vmem),
        scratch_shapes=[
            pltpu.VMEM((tokens, width), BF),
            pltpu.VMEM(cq.shape, BF),
            pltpu.VMEM(cv.shape, BF),
            pltpu.VMEM((rows, cols), F32),
            pltpu.VMEM((rows, cols), BF),
            pltpu.VMEM((2, tokens, rank), BF),
            pltpu.VMEM((rank, cols), BF),
            pltpu.VMEM((nr - 1, own, cols), BF),
            pltpu.VMEM((nz, own, cols), BF),
            pltpu.VMEM((2, 8, 128), F32),
            dma((7,)),
            dma((nz - 1,)),
            dma((nz - 1,)),
            dma((nz - 1,)),
            dma((nz - 1,)),
            dma(((nz - 1) * (nr - 1),)),
            dma(((nz - 1) * (nr - 1),)),
            dma((nz - 1, 4)),
            dma((nz - 1, 4)),
            dma((nr - 1,)),
            dma((nr - 1,)),
            dma((nz - 1,)),
            dma((nz - 1,)),
            dma((nr - 1,)),
            dma((nr - 1,)),
            dma((3,)),
            dma((3,)),
        ],
        compiler_params=pltpu.CompilerParams(
            collective_id=0, has_side_effects=True, vmem_limit_bytes=48 * 1024 * 1024
        ),
    )(x, cq, cv, wq, wv, qf, vf, q1, q2, v1, v2)


def local(
    nz,
    nr,
    saved_inputs,
    query_cotangent,
    value_cotangent,
    query_weight,
    value_weight,
    query_factor,
    value_factor,
    query_first,
    query_second,
    value_first,
    value_second,
):
    qc = query_cotangent.shape[1]
    rows = query_weight.shape[0]
    weights, factors, ratio, first, second, scale = run_exchange(
        nz,
        nr,
        saved_inputs,
        query_cotangent,
        value_cotangent,
        query_weight,
        value_weight,
        query_factor,
        value_factor,
        query_first,
        query_second,
        value_first,
        value_second,
    )
    query_scale = scale[0, 0]
    value_scale = scale[1, 0]
    query_raw = jnp.dot(factors[0], ratio[:, :qc], preferred_element_type=F32)
    value_raw = jnp.dot(factors[1], ratio[:, qc:], preferred_element_type=F32)
    query_copy = (weights[:, :qc].astype(F32) - RATE * (query_raw * query_scale)).astype(BF)
    value_copy = (weights[:, qc:].astype(F32) - RATE * (value_raw * value_scale)).astype(BF)
    query_direction = query_scale * jnp.dot(
        query_factor, ratio[:, :qc], preferred_element_type=F32
    )
    value_direction = value_scale * jnp.dot(
        value_factor, ratio[:, qc:], preferred_element_type=F32
    )
    query_master = query_weight - RATE * query_direction
    value_master = value_weight - RATE * value_direction
    return (
        query_direction,
        value_direction,
        query_master,
        value_master,
        first[:, :qc],
        second[:, :qc],
        first[:, qc:],
        second[:, qc:],
        query_copy,
        value_copy,
    )


def solution(mesh):
    return jax.shard_map(
        functools.partial(local, mesh.shape["fs"], mesh.shape["rep"]),
        mesh=mesh,
        in_specs=(
            P(("fs", "rep"), None),
            P(("fs", "rep"), "tp"),
            P(("fs", "rep"), "tp"),
            P("fs", "tp"),
            P("fs", "tp"),
            P("fs", None),
            P("fs", None),
            P("rep", "tp"),
            P("rep", "tp"),
            P("rep", "tp"),
            P("rep", "tp"),
        ),
        out_specs=(
            P("fs", "tp"),
            P("fs", "tp"),
            P("fs", "tp"),
            P("fs", "tp"),
            P("rep", "tp"),
            P("rep", "tp"),
            P("rep", "tp"),
            P("rep", "tp"),
            P(None, "tp"),
            P(None, "tp"),
        ),
        check_vma=False,
    )
```

time: 285 us -> 155 us (0.54); the launches traced: 280 us -> 154 us
  waiting for transfers between devices: 186 us -> 0 us
  Pallas kernels: 0 us -> 110 us
  blocking collectives: 37.5 us -> 0 us
  other arithmetic: 27 us -> 0 us
  local copies, waits for them, and re-layouts: 0.03 us -> 25.2 us
  between operations: 15.2 us -> 0.68 us
  matrix products: 14.4 us -> 19 us
    all_gather x2 -> x0, waiting for transfers between devices: 159 us -> none  [the longest x1 113 us: local(): lax.all_gather(jnp.concatenate([query_weight.astype(bf), value_weight.ast...]
    pallas_call x0 -> x1, Pallas kernels: none -> 110 us  [run_exchange(): pl.pallas_call(functools.partial(exchange, nz, nr), out_shape=(shape((wid...]
    reduce_scatter x1 -> x0, waiting for transfers between devices: 27 us -> none  [local(): lax.psum_scatter(proj.astype(bf), 'rep', scatter_dimension=0, tiled=True)]
    psum x2 -> x0, blocking collectives: 26.5 us -> none  [the longest x1 23.4 us: local(): proj = lax.psum(proj.astype(f32), 'fs')]
    unnamed x12 -> x30, local copies, waits for them, and re-layouts: 0.03 us -> 21.9 us
    convert_element_type x4 -> x0, other arithmetic: 14.6 us -> none  [the longest x1 5.67 us: local(): (weights[:, qc:].astype(f32) - RATE * (value_raw * value_scale)).astype(bf)]
    all_gather x1 -> x0, blocking collectives: 11 us -> none  [local(): ratio = lax.all_gather(ratio, 'rep', axis=0, tiled=True)]
    sub x2 -> x0, other arithmetic: 8.21 us -> none  [the longest x1 4.56 us: local(): value_master = value_weight - RATE * value_direction]
  transfers between devices with their start and end apart: 3 -> 0, of which waited for: 3 -> 0; matrix products, arithmetic and copies ran while one was open for 0% -> 0% of each run, Pallas kernels for 0% -> 0%
where the time goes in v2:
time: 155 us; the launch traced here: 154 us
  Pallas kernels  110 us (71%)
  local copies, waits for them, and re-layouts  25.2 us (16%)
  matrix products  19 us (12%)
    pallas_call x1, Pallas kernels, run_exchange(): pl.pallas_call(functools.partial(exchange, nz, nr), out_shape=(shape((wid...  110 us
    unnamed x30, local copies, waits for them, and re-layouts  21.9 us
    dot_general x1, matrix products, local(): value_raw = jnp.dot(factors[1], ratio[:, qc:], preferred_element_type=F32)  6.7 us
    dot_general x1, matrix products, local(): jnp.dot(value_factor, ratio[:, qc:], preferred_element_type=F32)  4.76 us
    dot_general x1, matrix products, local(): query_raw = jnp.dot(factors[0], ratio[:, :qc], preferred_element_type=F32)  4.33 us
    dot_general x1, matrix products, local(): jnp.dot(query_factor, ratio[:, :qc], preferred_element_type=F32)  3.19 us

profile of v2, /device:TPU:24, one launch (start us, length us, event | category | flops | bytes accessed | tf_op | source)
XLA Modules:
  0.0 154.5 jit_solution(103791972366782410)
XLA Ops:
  0.6 0.0 copy-start
  0.7 1.2 copy-done
  1.9 0.0 copy-start.2
  1.9 0.9 copy-done.2
  2.8 0.0 copy-start.4
  2.8 0.9 copy-done.4
  3.8 0.0 copy-start.6
  3.8 1.1 copy-done.6
  4.9 0.9 copy-done.7
  5.9 0.9 copy-done.8
  6.8 0.9 copy-done.9
  7.7 0.9 copy-done.10
  8.6 109.7 %shard_map.186 = (bf16[2048,1536]{1,0:T(8,128)(2,1)}, bf16[2,2048,256]{2,1,0:T(8,128)(2,1)}, bf16[256,1536]{1,0:T(8,128)(2,1)S(1)}, f32[64,1536]{1,0:T(8,128)S(1...) custom-call(bf16[768,2048]{1,0:T(8,128)(2,1)} %x_hbm.1, bf16[768,512]{1,0:T(8,128)(2,1)S(1)} %copy-done.6, ...), custom_call_target="tpu_custom_call" | custom-call | tf_op jit(solution)/shard_map/pallas_call | solution.py:328
  118.3 0.5 fusion.9
  118.8 6.7 %subtract_convert_fusion = bf16[2048,1024]{1,0:T(8,128)(2,1)} fusion(f32[]{:T(128)} %bitcast.2, bf16[2048,1536]{1,0:T(8,128)(2,1)} %get-tuple-element.20, bf16[2,2048,256]{2,1,0:T(8,128)(2,1)} %get-tuple-element.21, bf16[256,1536]{1,0:T(8,128)(2,1)S(1)} %get-tuple-element.17), kind=kOutput, calls=%fused_computation | convolution fusion | flops 1084227584 | bytes 9961984 | tf_op jit(solution)/shard_map/dot_general | solution.py:410
  125.5 0.0 copy-done.11
  125.5 4.3 %subtract_convert_fusion.1 = bf16[2048,512]{1,0:T(8,128)(2,1)} fusion(f32[]{:T(128)} %bitcast, bf16[2048,1536]{1,0:T(8,128)(2,1)} %get-tuple-element.20, bf16[2,2048,256]{2,1,0:T(8,128)(2,1)S(1)} %copy-done.11, bf16[256,1536]{1,0:T(8,128)(2,1)S(1)} %get-tuple-element.17), kind=kOutput, calls=%fused_computation.1 | convolution fusion | flops 542113792 | bytes 5505028 | tf_op jit(solution)/shard_map/dot_general | solution.py:409
  129.8 2.9 %copy.22 = f32[512,1024]{0,1:T(8,128)} copy(f32[512,1024]{1,0:T(8,128)} %wv_hbm.1) | data formatting | bytes 4194304 | tf_op args[4]
  132.8 0.0 copy-done.3
  132.8 4.8 %multiply_subtract_fusion = (f32[512,1024]{0,1:T(8,128)}, f32[512,1024]{0,1:T(8,128)}) fusion(f32[512,1024]{0,1:T(8,128)} %copy.22, bf16[512,256]{1,0:T(8,128)(2,1)S(1)} %copy-done.3, bf16[256,1536]{1,0:T(8,128)(2,1)S(1)} %get-tuple-element.17, f32[]{:T(128)} %bitcast.2), kind=kOutput, calls=%fused_computation.2 | convolution fusion | flops 270008320 | bytes 7077892 | tf_op jit(solution)/shard_map/dot_general | solution.py:416
  137.5 2.9 %copy.24 = f32[512,1024]{1,0:T(8,128)} copy(f32[512,1024]{0,1:T(8,128)} %get-tuple-element.37) | data formatting | bytes 4194304
  140.4 3.0 %copy.26 = f32[512,1024]{1,0:T(8,128)} copy(f32[512,1024]{0,1:T(8,128)} %get-tuple-element.36) | data formatting | bytes 4194304
  143.4 0.0 copy-done.1
  143.4 1.3 copy.21
  144.7 0.0 copy-done.5
  144.7 3.2 %multiply_subtract_fusion.1 = (f32[512,512]{0,1:T(8,128)S(1)}, f32[512,512]{0,1:T(8,128)}) fusion(f32[512,512]{0,1:T(8,128)} %copy.21, bf16[512,256]{1,0:T(8,128)(2,1)S(1)} %copy-done.5, bf16[256,1536]{1,0:T(8,128)(2,1)S(1)} %get-tuple-element.17, f32[]{:T(128)} %bitcast), kind=kOutput, calls=%fused_computation.10 | convolution fusion | flops 135004160 | bytes 3670020 | tf_op jit(solution)/shard_map/dot_general | solution.py:413
  147.9 2.5 %copy.23 = f32[512,512]{1,0:T(8,128)} copy(f32[512,512]{0,1:T(8,128)} %get-tuple-element.35) | data formatting | bytes 2097152
  150.4 1.3 copy.25
  151.7 0.7 slice.44
  152.4 0.7 slice.45
  153.2 0.7 slice.42
  153.8 0.7 slice.43
  (8 shorter events, 0.0 us)
Async XLA Ops:
  0.6 1.2 copy-start
  1.9 0.9 copy-start.2
  2.8 0.9 copy-start.4
  3.8 1.1 copy-start.6
  4.9 0.9 copy-start.7
  5.9 0.9 copy-start.8
  6.8 0.9 copy-start.9
  7.7 0.9 copy-start.10
  118.8 6.7 %copy-start.11 = (bf16[2,2048,256]{2,1,0:T(8,128)(2,1)S(1)}, bf16[2,2048,256]{2,1,0:T(8,128)(2,1)}, u32[]{:S(2)}) copy-start(bf16[2,2048,256]{2,1,0:T(8,128)(2,1)} %get-tuple-element.21) | copy-start | bytes 6291460
  129.8 2.9 %copy-start.3 = (bf16[512,256]{1,0:T(8,128)(2,1)S(1)}, bf16[512,256]{1,0:T(8,128)(2,1)}, u32[]{:S(2)}) copy-start(bf16[512,256]{1,0:T(8,128)(2,1)} %vf_hbm.1) | copy-start | bytes 786436
  140.4 3.0 %copy-start.1 = (f32[512,512]{1,0:T(8,128)S(1)}, f32[512,512]{1,0:T(8,128)}, u32[]{:S(2)}) copy-start(f32[512,512]{1,0:T(8,128)} %wq_hbm.1) | copy-start | bytes 3145732
  143.4 1.3 copy-start.5

commit v3 on v2

--- a/solution.py
+++ b/solution.py
@@ -33,15 +33,14 @@
     wv_hbm,
     qf_hbm,
     vf_hbm,
-    q1_ref,
-    q2_ref,
-    v1_ref,
-    v2_ref,
+    q1_hbm,
+    q2_hbm,
+    v1_hbm,
+    v2_hbm,
     w_out,
     f_ref,
     ratio_ref,
-    first_out,
-    second_out,
+    proj_out,
     scale_out,
     x_ref,
     cq_ref,
@@ -52,6 +51,10 @@
     part_ref,
     rs_ref,
     z_ref,
+    zg_ref,
+    zh_ref,
+    m1_ref,
+    m2_ref,
     sq_ref,
     local_sem,
     f1_s,
@@ -66,6 +69,8 @@
     rs_r,
     zs_s,
     zs_r,
+    zg_s,
+    zg_r,
     ag_s,
     ag_r,
     tp_s,
@@ -124,7 +129,19 @@
     x_in = pltpu.make_async_copy(x_hbm, x_ref, local_sem.at[3])
     cq_in = pltpu.make_async_copy(cq_hbm, cq_ref, local_sem.at[4])
     cv_in = pltpu.make_async_copy(cv_hbm, cv_ref, local_sem.at[5])
-    for c in (wq_in, wv_in, x_in, cq_in, cv_in):
+    left, right = pl.ds(0, qc), pl.ds(qc, cols - qc)
+    mom = [
+        pltpu.make_async_copy(src, dst.at[:, at], local_sem.at[7 + n])
+        for n, (src, dst, at) in enumerate(
+            (
+                (q1_hbm, m1_ref, left),
+                (v1_hbm, m1_ref, right),
+                (q2_hbm, m2_ref, left),
+                (v2_hbm, m2_ref, right),
+            )
+        )
+    ]
+    for c in [wq_in, wv_in, x_in, cq_in, cv_in] + mom:
         c.start()
 
     barrier = pltpu.get_barrier_semaphore()
@@ -175,6 +192,31 @@
             f2.append(c)
     for c in f2:
         c.wait_recv()
+    w2 = {}
+
+    def spread(k):
+        w1[k - 1].wait_recv()
+        there = w_out.at[slab(z_from[k], r)]
+        for n, dev in ((0, side), (1, over)):
+            c = remote(there, there, w2_s.at[k - 1, n], w2_r.at[k - 1, n], (z, dev, t))
+            c.start()
+            w2[k, n] = c
+
+    def relay(k):
+        for n, src, dev, at in ((0, side, over, 0), (1, over, side, half)):
+            w2[k, n].wait_recv()
+            there = w_out.at[slab(z_from[k], src), pl.ds(at, half)]
+            c = remote(
+                there, there, w2_s.at[k - 1, 2 + n], w2_r.at[k - 1, 2 + n], (z, dev, t)
+            )
+            c.start()
+            w2[k, 2 + n] = c
+
+    stages = [[], [], []]
+    for k in range(1, nz):
+        stages[min(k - 1, 2)].append(k)
+    for k in stages[0]:
+        spread(k)
     fx = remote(f_ref.at[t], f_ref.at[t], tp_s.at[0], tp_r.at[0], (z, r, other))
     fx.start()
     x_in.wait()
@@ -215,69 +257,70 @@
         c.start()
         rsc.append(c)
 
-    w2 = {}
-
-    def spread(k):
-        w1[k - 1].wait_recv()
-        there = w_out.at[slab(z_from[k], r)]
-        for n, dev in ((0, side), (1, over)):
-            c = remote(there, there, w2_s.at[k - 1, n], w2_r.at[k - 1, n], (z, dev, t))
-            c.start()
-            w2[k, n] = c
-
-    def relay(k):
-        for n, src, dev, at in ((0, side, over, 0), (1, over, side, half)):
-            w2[k, n].wait_recv()
-            there = w_out.at[slab(z_from[k], src), pl.ds(at, half)]
-            c = remote(
-                there, there, w2_s.at[k - 1, 2 + n], w2_r.at[k - 1, 2 + n], (z, dev, t)
-            )
-            c.start()
-            w2[k, 2 + n] = c
-
-    stages = [[], [], []]
-    for k in range(1, nz):
-        stages[min(k - 1, 2)].append(k)
+    for k in stages[0]:
+        relay(k)
     for c in rsc:
         c.wait_recv()
     total = part_ref[low_rows(r), :].astype(F32)
     for j in range(1, nr):
         total = total + rs_ref[j - 1].astype(F32)
-    z_ref[z] = total.astype(BF)
+    share = own // nz
+    scatter = share % 16 == 0
     zc = []
-    for k in range(1, nz):
-        c = remote(z_ref.at[z], z_ref.at[z], zs_s.at[k - 1], zs_r.at[k - 1], (z_of[k], r, t))
+    if scatter:
+        zg_ref[...] = total.astype(BF)
+    else:
+        z_ref[z] = total.astype(BF)
+
+    def z_rows(zz):
+        return pl.ds(pl.multiple_of(zz * share, share), share)
+
+    for k in range(1, nz):
+        src = zg_ref.at[z_rows(z_of[k])] if scatter else z_ref.at[z]
+        c = remote(src, z_ref.at[z], zs_s.at[k - 1], zs_r.at[k - 1], (z_of[k], r, t))
         c.start()
         zc.append(c)
-    for k in stages[0]:
+    if scatter:
+        z_ref[z] = zg_ref[z_rows(z), :]
+    for k in stages[1]:
         spread(k)
     for c in zc:
         c.wait_recv()
     proj = z_ref[0].astype(F32)
     for k in range(1, nz):
         proj = proj + z_ref[k].astype(F32)
-    q1, q2, qr = moments(proj[:, :qc], q1_ref[...], q2_ref[...])
-    v1, v2, vr = moments(proj[:, qc:], v1_ref[...], v2_ref[...])
-    ratio_ref[low_rows(r), :qc] = qr.astype(BF)
-    ratio_ref[low_rows(r), qc:] = vr.astype(BF)
+    gc = []
+    if scatter:
+        for c in zc:
+            c.wait_send()
+        zh = zh_ref
+        zh[z_rows(z), :] = proj.astype(BF)
+        for k in range(1, nz):
+            here = zh.at[z_rows(z)]
+            c = remote(here, here, zg_s.at[k - 1], zg_r.at[k - 1], (z_of[k], r, t))
+            c.start()
+            gc.append(c)
+    for k in stages[1]:
+        relay(k)
+    for k in stages[2]:
+        spread(k)
+    for c in mom:
+        c.wait()
+    if scatter:
+        for c in gc:
+            c.wait_recv()
+        proj = zh[...].astype(F32)
+    proj_out[...] = proj
+    _, _, ratio = moments(proj, m1_ref[...], m2_ref[...])
+    ratio_ref[low_rows(r), :] = ratio.astype(BF)
     agc = []
     for j in range(1, nr):
         here = ratio_ref.at[low_rows(r)]
         c = remote(here, here, ag_s.at[j - 1], ag_r.at[j - 1], (z, r_of[j], t))
         c.start()
         agc.append(c)
-    first_out[:, :qc] = q1
-    first_out[:, qc:] = v1
-    second_out[:, :qc] = q2
-    second_out[:, qc:] = v2
-    for k in stages[0]:
+    for k in stages[2]:
         relay(k)
-    for k in stages[1]:
-        spread(k)
-    for k in stages[1]:
-        relay(k)
-    for k in stages[2]:
-        spread(k)
     fx.wait_recv()
     for c in agc:
         c.wait_recv()
@@ -305,12 +348,10 @@
     sx.start()
     sx.wait_recv()
     scale_out[...] = lax.rsqrt(sq_ref[0] + sq_ref[1] + EPS_NORM)
-    for k in stages[2]:
-        relay(k)
     for k in range(1, nz):
         w2[k, 2].wait_recv()
         w2[k, 3].wait_recv()
-    for c in f1 + w1 + f2 + rsc + zc + agc + [fx, lx, sx] + list(w2.values()):
+    for c in f1 + w1 + f2 + rsc + ([] if scatter else zc) + gc + agc + [fx, lx, sx] + list(w2.values()):
         c.wait_send()
     w_own.wait()
 
@@ -321,7 +362,8 @@
     cols = qc + cv.shape[1]
     rows, rank = qf.shape
     own = rank // nr
-    any_spec = pl.BlockSpec(memory_space=pl.ANY)
+    share = own // nz if (own // nz) % 16 == 0 else own
+    any_spec = pl.BlockSpec(memory_space=pltpu.HBM)
     vmem = pl.BlockSpec(memory_space=pltpu.VMEM)
     dma = pltpu.SemaphoreType.DMA
     shape = jax.ShapeDtypeStruct
@@ -332,11 +374,10 @@
             shape((2, width, rank), BF),
             shape((rank, cols), BF),
             shape((own, cols), F32),
-            shape((own, cols), F32),
             shape((8, 128), F32),
         ),
-        in_specs=[any_spec] * 7 + [vmem] * 4,
-        out_specs=(any_spec, vmem, vmem, vmem, vmem, vmem),
+        in_specs=[any_spec] * 11,
+        out_specs=(any_spec, vmem, vmem, vmem, vmem),
         scratch_shapes=[
             pltpu.VMEM((tokens, width), BF),
             pltpu.VMEM(cq.shape, BF),
@@ -346,9 +387,13 @@
             pltpu.VMEM((2, tokens, rank), BF),
             pltpu.VMEM((rank, cols), BF),
             pltpu.VMEM((nr - 1, own, cols), BF),
-            pltpu.VMEM((nz, own, cols), BF),
+            pltpu.VMEM((nz, share, cols), BF),
+            pltpu.VMEM((own, cols), BF),
+            pltpu.VMEM((own, cols), BF),
+            pltpu.VMEM((own, cols), F32),
+            pltpu.VMEM((own, cols), F32),
             pltpu.VMEM((2, 8, 128), F32),
-            dma((7,)),
+            dma((11,)),
             dma((nz - 1,)),
             dma((nz - 1,)),
             dma((nz - 1,)),
@@ -361,74 +406,137 @@
             dma((nr - 1,)),
             dma((nz - 1,)),
             dma((nz - 1,)),
+            dma((nz - 1,)),
+            dma((nz - 1,)),
             dma((nr - 1,)),
             dma((nr - 1,)),
             dma((3,)),
             dma((3,)),
         ],
         compiler_params=pltpu.CompilerParams(
-            collective_id=0, has_side_effects=True, vmem_limit_bytes=48 * 1024 * 1024
+            collective_id=0, has_side_effects=True, vmem_limit_bytes=60 * 1024 * 1024
         ),
     )(x, cq, cv, wq, wv, qf, vf, q1, q2, v1, v2)
 
 
-def local(
-    nz,
-    nr,
-    saved_inputs,
-    query_cotangent,
-    value_cotangent,
-    query_weight,
-    value_weight,
-    query_factor,
-    value_factor,
-    query_first,
-    query_second,
-    value_first,
-    value_second,
+def finish(
+    f_ref,
+    ratio_ref,
+    scale_ref,
+    w_ref,
+    wq_ref,
+    wv_ref,
+    qf_ref,
+    vf_ref,
+    proj_ref,
+    q1_ref,
+    q2_ref,
+    v1_ref,
+    v2_ref,
+    qd_out,
+    vd_out,
+    qm_out,
+    vm_out,
+    q1_out,
+    q2_out,
+    v1_out,
+    v2_out,
+    qcopy_out,
+    vcopy_out,
 ):
-    qc = query_cotangent.shape[1]
-    rows = query_weight.shape[0]
-    weights, factors, ratio, first, second, scale = run_exchange(
-        nz,
-        nr,
-        saved_inputs,
-        query_cotangent,
-        value_cotangent,
-        query_weight,
-        value_weight,
-        query_factor,
-        value_factor,
-        query_first,
-        query_second,
-        value_first,
-        value_second,
+    qc = wq_ref.shape[1]
+    sets = (
+        (0, pl.ds(0, qc), wq_ref, qf_ref, q1_ref, q2_ref, qd_out, qm_out, q1_out, q2_out, qcopy_out),
+        (
+            1,
+            pl.ds(qc, wv_ref.shape[1]),
+            wv_ref,
+            vf_ref,
+            v1_ref,
+            v2_ref,
+            vd_out,
+            vm_out,
+            v1_out,
+            v2_out,
+            vcopy_out,
+        ),
     )
-    query_scale = scale[0, 0]
-    value_scale = scale[1, 0]
-    query_raw = jnp.dot(factors[0], ratio[:, :qc], preferred_element_type=F32)
-    value_raw = jnp.dot(factors[1], ratio[:, qc:], preferred_element_type=F32)
-    query_copy = (weights[:, :qc].astype(F32) - RATE * (query_raw * query_scale)).astype(BF)
-    value_copy = (weights[:, qc:].astype(F32) - RATE * (value_raw * value_scale)).astype(BF)
-    query_direction = query_scale * jnp.dot(
-        query_factor, ratio[:, :qc], preferred_element_type=F32
-    )
-    value_direction = value_scale * jnp.dot(
-        value_factor, ratio[:, qc:], preferred_element_type=F32
-    )
-    query_master = query_weight - RATE * query_direction
-    value_master = value_weight - RATE * value_direction
-    return (
-        query_direction,
-        value_direction,
-        query_master,
-        value_master,
-        first[:, :qc],
-        second[:, :qc],
-        first[:, qc:],
-        second[:, qc:],
-        query_copy,
-        value_copy,
+    for n, at, w, f, m1, m2, d_out, m_out, m1_out, m2_out, c_out in sets:
+        scale = scale_ref[n : n + 1, 0:1]
+        ratio = ratio_ref[:, at]
+        raw = jnp.dot(f_ref[n], ratio, preferred_element_type=F32)
+        c_out[...] = (w_ref[:, at].astype(F32) - RATE * (raw * scale)).astype(BF)
+        d = jnp.dot(f[...], ratio, preferred_element_type=F32) * scale
+        d_out[...] = d
+        m_out[...] = w[...] - RATE * d
+        m1_out[...], m2_out[...], _ = moments(proj_ref[:, at], m1[...], m2[...])
+
+
+def run_finish(factors, ratio, scale, weights, wq, wv, qf, vf, proj, q1, q2, v1, v2):
+    rows, qc = wq.shape
+    vc = wv.shape[1]
+    width, cols = weights.shape
+    rank, own = qf.shape[1], q1.shape[0]
+    steps = 8 if rows % 128 == 0 else 4
+
+    def tall(n, c):
+        return pl.BlockSpec((n // steps, c), lambda i: (i, 0))
+
+    def whole(a):
+        return pl.BlockSpec(a.shape, lambda i: (0,) * a.ndim)
+
+    shape = jax.ShapeDtypeStruct
+    return pl.pallas_call(
+        finish,
+        grid=(steps,),
+        in_specs=[
+            pl.BlockSpec((2, width // steps, rank), lambda i: (0, i, 0)),
+            whole(ratio),
+            whole(scale),
+            tall(width, cols),
+            tall(rows, qc),
+            tall(rows, vc),
+            tall(rows, rank),
+            tall(rows, rank),
+            tall(own, cols),
+            tall(own, qc),
+            tall(own, qc),
+            tall(own, vc),
+            tall(own, vc),
+        ],
+        out_specs=[
+            tall(rows, qc),
+            tall(rows, vc),
+            tall(rows, qc),
+            tall(rows, vc),
+            tall(own, qc),
+            tall(own, qc),
+            tall(own, vc),
+            tall(own, vc),
+            tall(width, qc),
+            tall(width, vc),
+        ],
+        out_shape=[
+            shape((rows, qc), F32),
+            shape((rows, vc), F32),
+            shape((rows, qc), F32),
+            shape((rows, vc), F32),
+            shape((own, qc), F32),
+            shape((own, qc), F32),
+            shape((own, vc), F32),
+            shape((own, vc), F32),
+            shape((width, qc), BF),
+            shape((width, vc), BF),
+        ],
+        compiler_params=pltpu.CompilerParams(vmem_limit_bytes=60 * 1024 * 1024),
+    )(factors, ratio, scale, weights, wq, wv, qf, vf, proj, q1, q2, v1, v2)
+
+
+def local(nz, nr, *args):
+    _, _, _, wq, wv, qf, vf, q1, q2, v1, v2 = args
+    weights, factors, ratio, proj, scale = run_exchange(nz, nr, *args)
+    return tuple(
+        run_finish(factors, ratio, scale, weights, wq, wv, qf, vf, proj, q1, q2, v1, v2)
     )
 
 

time: 155 us -> 110 us (0.71)
  the two profiles are of different devices: /device:TPU:24 before, /device:TPU:17 now
where the time goes in v3:
time: 110 us; the launch traced here: 109 us
  Pallas kernels  109 us (99%)
    pallas_call x1, Pallas kernels, run_exchange(): pl.pallas_call(functools.partial(exchange, nz, nr), out_shape=(shape((wid...  95.7 us
    pallas_call x1, Pallas kernels, run_finish(): pl.pallas_call(finish, grid=(steps,), in_specs=[pl.BlockSpec((2, width //...  12.9 us

profile of v3, /device:TPU:17, one launch (start us, length us, event | category | flops | bytes accessed | tf_op | source)
XLA Modules:
  0.0 109.3 jit_solution(15235253364751065104)
XLA Ops:
  0.6 95.7 %shard_map.186 = (bf16[2048,1536]{1,0:T(8,128)(2,1)}, bf16[2,2048,256]{2,1,0:T(8,128)(2,1)}, bf16[256,1536]{1,0:T(8,128)(2,1)}, f32[64,1536]{1,0:T(8,128)}, f32[8,128]{1,0:T(8,128)}) custom-call(bf16[768,2048]{1,0:T(8,128)(2,1)} %x_hbm.1, bf16[768,512]{1,0:T(8,128)(2,1)} %cq_hbm.1, bf16[768,1024]{1,0:T(8,128)(2,1)} %cv_hbm.1, f32[512,512]{1,0:T(8,128)} %wq_ref.1, ...), custom_call_target="tpu_custom_call" | custom-call | tf_op jit(solution)/shard_map/pallas_call | solution.py:370
  96.3 12.9 %shard_map.187 = (f32[512,512]{1,0:T(8,128)}, f32[512,1024]{1,0:T(8,128)}, f32[512,512]{1,0:T(8,128)}, f32[512,1024]{1,0:T(8,128)}, f32[64,512]{1,0:T(8,128)}, /...) custom-call(bf16[2,2048,256]{2,1,0:T(8,128)(2,1)} %get-tuple-element, ...), custom_call_target="tpu_custom_call" | custom-call | tf_op jit(solution)/shard_map/pallas_call | solution.py:489
